TPU v7x, 32 devices: a whole 2x2x4 slice. The times are simulated.
32 devices in a mesh: sp: 4 (over z), tp: 8 (over y, x, core).
Axes of the slice: x: 2, y: 2, z: 4, core: 2. Of those that a mesh axis runs over, the one named last changes fastest.
Arguments:
- stream: bfloat16 [1024, 4096], P('sp', 'tp'), may hold values from -80 to 80
- norm_gain: bfloat16 [3, 4096], replicated, may hold values from 0.099609375 to 1.8984375
- value_weight: bfloat16 [3, 2048, 4096], P(None, 'tp'), may hold values from -0.09375 to 0.09375
- gate_weight: bfloat16 [3, 2048, 4096], P(None, 'tp'), may hold values from -0.09375 to 0.09375
- kernel: float32 [3, 31, 2048], P(None, None, 'tp'), may hold values from -8 to 8
- kernel_bias: float32 [3, 2048], P(None, 'tp'), may hold values from -3 to 3
- chan_gain: float32 [3, 2048], P(None, 'tp'), may hold values from 0.1 to 1.9
- chan_shift: float32 [3, 2048], P(None, 'tp'), may hold values from -3 to 3
- out_weight: bfloat16 [3, 2048, 4096], P(None, None, 'tp'), may hold values from -0.125 to 0.125
Outputs:
- result: bfloat16 [1024, 4096], P('sp', 'tp')
All inputs are finite; a program needn't handle non-finite values.
Results may differ from a plain program's by a relative error of at most 0.012.
Values may be sent and summed in bfloat16 or wider, within the bound.
A program may use at most 64 MiB of HBM per device.

v0:
```python
import jax
import jax.numpy as jnp
from jax import lax
from jax.sharding import PartitionSpec as P

EPSILON = 1e-06


def passed_along(shard, axis, by):
    count = lax.axis_size(axis)
    pairs = [(i, i + by) for i in range(count) if 0 <= i + by < count]
    return lax.ppermute(shard, axis, pairs)


def against(left, right):
    return lax.dot_general(
        left, right, (((1,), (1,)), ((), ())), preferred_element_type=jnp.float32
    )


def on_device(
    stream,
    norm_gain,
    value_weight,
    gate_weight,
    kernel,
    kernel_bias,
    chan_gain,
    chan_shift,
    out_weight,
):
    layer_count = kernel.shape[0]
    reach_back = kernel.shape[1] - 1
    local_width = stream.shape[1]
    channels = kernel.shape[2] * lax.axis_size("tp")
    current = stream
    for layer_at in range(layer_count):
        gain_row = norm_gain[layer_at].astype(jnp.float32)
        value_matrix = value_weight[layer_at]
        gate_matrix = gate_weight[layer_at]
        row_count = current.shape[0]
        whole_rows = lax.all_gather(current, "tp", axis=1, tiled=True)
        whole_float = whole_rows.astype(jnp.float32)
        scale_row = lax.rsqrt(jnp.mean(whole_float * whole_float, axis=1, keepdims=True) + EPSILON)
        normed = (whole_float * scale_row * gain_row[None, :]).astype(jnp.bfloat16)
        value_part = against(normed, value_matrix)
        gate_part = against(normed, gate_matrix)
        gated_rows = (value_part * jax.nn.sigmoid(gate_part)).astype(jnp.bfloat16)
        earlier_taps = passed_along(gated_rows[row_count - reach_back :], "sp", 1)
        padded = jnp.concatenate([earlier_taps, gated_rows], axis=0)
        out_rows = padded.shape[0] - reach_back
        kernel_now = kernel[layer_at]
        convolved = jnp.broadcast_to(
            kernel_bias[layer_at][None, :], (out_rows, kernel_now.shape[1])
        )
        for tap_at in range(reach_back + 1):
            convolved = convolved + kernel_now[tap_at][None, :] * padded[
                tap_at : tap_at + out_rows
            ].astype(jnp.float32)
        totals = lax.psum(
            (jnp.sum(convolved, axis=1), jnp.sum(convolved * convolved, axis=1)), "tp"
        )
        centre = totals[0] / channels
        spread = totals[1] / channels - centre * centre
        normal_out = (convolved - centre[:, None]) * lax.rsqrt(spread + EPSILON)[
            :, None
        ] * chan_gain[layer_at][None, :] + chan_shift[layer_at][None, :]
        hidden = jax.nn.silu(normal_out).astype(jnp.bfloat16)
        out_matrix = out_weight[layer_at]

        def project_out(running, block_in, offset_at, out_matrix=out_matrix):
            return jnp.dot(block_in, out_matrix, preferred_element_type=jnp.float32)

        projected = project_out(
            jnp.zeros((out_rows, local_width), jnp.float32),
            lax.all_gather(hidden, "tp", axis=1, tiled=True),
            jnp.int32(0),
        )
        current = (current.astype(jnp.float32) + projected).astype(jnp.bfloat16)
    return current


def solution(mesh):
    return jax.shard_map(
        on_device,
        mesh=mesh,
        in_specs=(
            P("sp", "tp"),
            P(),
            P(None, "tp", None),
            P(None, "tp", None),
            P(None, None, "tp"),
            P(None, "tp"),
            P(None, "tp"),
            P(None, "tp"),
            P(None, None, "tp"),
        ),
        out_specs=P("sp", "tp"),
        check_vma=False,
    )
```

profile of v0, /device:TPU:0, one launch (start us, length us, event | category | flops | bytes accessed | tf_op | source)
XLA Modules:
  0.0 266.8 jit_solution(3278399664090631594)
XLA Ops:
  8.9 1.0 fusion.208
  9.9 1.1 fusion.207
  12.0 28.1 %all-gather.7.cloned.1.call-done = bf16[256,4096]{1,0:T(8,128)(2,1)} async-done(((bf16[256,512]{1,0:T(8,128)(2,1)}), bf16[256,4096]{1,0:T(8,128)(2,1)}) %all-gather.7.cloned.1.call-update) | async-done | bytes 2097168 | tf_op jit(solution)/shard_map/all_gather | solution.py:42
  40.1 2.1 fusion
  42.2 3.2 %fusion.96 = f32[256,256]{1,0:T(8,128)S(1)} fusion(bf16[3,256,4096]{2,1,0:T(8,128)(2,1)} %param.12, bf16[256,4096]{1,0:T(8,128)(2,1)} %all-gather.7.cloned.1.call-done, f32[4096]{0:T(1024)S(1)} %bitcast.187, f32[256]{0:T(256)S(1)} %add_rsqrt_fusion.5), kind=kOutput, calls=%fused_computation.149 | convolution fusion | flops 541261824 | bytes 4473856 | tf_op jit(solution)/shard_map/dot_general | solution.py:16
  45.4 2.5 fusion.105
  47.9 3.5 %collective-permute-start = (bf16[30,256]{1,0:T(8,128)(2,1)S(1)}, bf16[30,256]{1,0:T(8,128)(2,1)S(1)}, u32[]{:S(2)}, u32[]{:S(2)}) collective-permute-start(bf16[30,256]{1,0:T(8,128)(2,1)S(1)} %slice.1017), channel_id=1, source_target_pairs={{0,8},{8,16},{16,24},{1,9},{9,17},{17,25},{2,10},{10,18},{18,26},{... | collective-permute-start | bytes 46088 | tf_op jit(solution)/shard_map/ppermute | solution.py:12
  51.4 1.4 collective-permute-done
  52.8 1.2 fusion.203
  54.0 12.2 %all-reduce.2 = (f32[256]{0:T(256)S(1)}, f32[256]{0:T(256)S(1)}) all-reduce(f32[256]{0:T(256)S(1)} %get-tuple-element.10, f32[256]{0:T(256)S(1)} %get-tuple-element.9), channel_id=1, replica_groups=mesh['sp'=4,'tp'=8] {'tp'}, use_global_device_ids=true, to_apply=%region_4.0 | all-reduce | flops 512 | bytes 4096 | tf_op jit(solution)/shard_map/psum | solution.py:60
  67.2 24.1 %all-gather.9.cloned.1.call-done = bf16[256,2048]{1,0:T(8,128)(2,1)} async-done(((bf16[256,256]{1,0:T(8,128)(2,1)}), bf16[256,2048]{1,0:T(8,128)(2,1)}) %all-gather.9.cloned.1.call-update) | async-done | bytes 1048592 | tf_op jit(solution)/shard_map/all_gather | solution.py:76
  91.3 3.3 %fusion.51 = bf16[256,512]{1,0:T(8,128)(2,1)} fusion(bf16[256,2048]{1,0:T(8,128)(2,1)} %all-gather.9.cloned.1.call-done, bf16[3,2048,512]{2,1,0:T(8,128)(2,1)} %param.17, bf16[256,512]{1,0:T(8,128)(2,1)S(1)} %copy-done.3), kind=kOutput, calls=%fused_computation.134 | convolution fusion | flops 537264128 | bytes 3670016 | tf_op jit(solution)/shard_map/dot_general | solution.py:72
  94.7 28.2 %all-gather.11.cloned.1.call-done = bf16[256,4096]{1,0:T(8,128)(2,1)} async-done(((bf16[256,512]{1,0:T(8,128)(2,1)}), bf16[256,4096]{1,0:T(8,128)(2,1)}) %all-gather.11.cloned.1.call-update) | async-done | bytes 2097168 | tf_op jit(solution)/shard_map/all_gather | solution.py:42
  122.9 2.1 fusion.3
  125.0 3.2 %fusion.93 = f32[256,256]{1,0:T(8,128)S(1)} fusion(bf16[3,256,4096]{2,1,0:T(8,128)(2,1)} %param.12, bf16[256,4096]{1,0:T(8,128)(2,1)} %all-gather.11.cloned.1.call-done, f32[4096]{0:T(1024)S(1)} %bitcast.185, f32[256]{0:T(256)S(1)} %add_rsqrt_fusion.3), kind=kOutput, calls=%fused_computation.148 | convolution fusion | flops 541261824 | bytes 4473856 | tf_op jit(solution)/shard_map/dot_general | solution.py:16
  128.2 2.4 fusion.102
  130.7 3.4 %collective-permute-start.1 = (bf16[30,256]{1,0:T(8,128)(2,1)S(1)}, bf16[30,256]{1,0:T(8,128)(2,1)S(1)}, u32[]{:S(2)}, u32[]{:S(2)}) collective-permute-start(bf16[30,256]{1,0:T(8,128)(2,1)S(1)} %slice.1076), channel_id=1, source_target_pairs={{0,8},{8,16},{16,24},{1,9},{9,17},{17,25},{2,10},{10,18},{18,26},{... | collective-permute-start | bytes 46088 | tf_op jit(solution)/shard_map/ppermute | solution.py:12
  134.1 1.4 collective-permute-done.1
  135.5 1.2 fusion.202
  136.7 12.2 %all-reduce.1 = (f32[256]{0:T(256)S(1)}, f32[256]{0:T(256)S(1)}) all-reduce(f32[256]{0:T(256)S(1)} %get-tuple-element.8, f32[256]{0:T(256)S(1)} %get-tuple-element.7), channel_id=1, replica_groups=mesh['sp'=4,'tp'=8] {'tp'}, use_global_device_ids=true, to_apply=%region_9.10 | all-reduce | flops 512 | bytes 4096 | tf_op jit(solution)/shard_map/psum | solution.py:60
  149.8 24.1 %all-gather.13.cloned.1.call-done = bf16[256,2048]{1,0:T(8,128)(2,1)} async-done(((bf16[256,256]{1,0:T(8,128)(2,1)}), bf16[256,2048]{1,0:T(8,128)(2,1)}) %all-gather.13.cloned.1.call-update) | async-done | bytes 1048592 | tf_op jit(solution)/shard_map/all_gather | solution.py:76
  173.9 3.3 %fusion.48 = bf16[256,512]{1,0:T(8,128)(2,1)} fusion(bf16[256,2048]{1,0:T(8,128)(2,1)} %all-gather.13.cloned.1.call-done, bf16[3,2048,512]{2,1,0:T(8,128)(2,1)} %param.17, bf16[256,512]{1,0:T(8,128)(2,1)S(1)} %copy-done.4), kind=kOutput, calls=%fused_computation.133 | convolution fusion | flops 537264128 | bytes 3670016 | tf_op jit(solution)/shard_map/dot_general | solution.py:72
  177.3 28.2 %all-gather.15.cloned.1.call-done = bf16[256,4096]{1,0:T(8,128)(2,1)} async-done(((bf16[256,512]{1,0:T(8,128)(2,1)}), bf16[256,4096]{1,0:T(8,128)(2,1)}) %all-gather.15.cloned.1.call-update) | async-done | bytes 2097168 | tf_op jit(solution)/shard_map/all_gather | solution.py:42
  205.6 2.1 fusion.6
  207.7 3.2 %fusion.90 = f32[256,256]{1,0:T(8,128)S(1)} fusion(bf16[3,256,4096]{2,1,0:T(8,128)(2,1)} %param.12, bf16[256,4096]{1,0:T(8,128)(2,1)} %all-gather.15.cloned.1.call-done, f32[4096]{0:T(1024)S(1)} %bitcast.183, f32[256]{0:T(256)S(1)} %add_rsqrt_fusion.1), kind=kOutput, calls=%fused_computation.147 | convolution fusion | flops 541261824 | bytes 4473856 | tf_op jit(solution)/shard_map/dot_general | solution.py:16
  210.8 2.5 fusion.99
  213.3 3.4 %collective-permute-start.2 = (bf16[30,256]{1,0:T(8,128)(2,1)S(1)}, bf16[30,256]{1,0:T(8,128)(2,1)S(1)}, u32[]{:S(2)}, u32[]{:S(2)}) collective-permute-start(bf16[30,256]{1,0:T(8,128)(2,1)S(1)} %slice.1135), channel_id=1, source_target_pairs={{0,8},{8,16},{16,24},{1,9},{9,17},{17,25},{2,10},{10,18},{18,26},{... | collective-permute-start | bytes 46088 | tf_op jit(solution)/shard_map/ppermute | solution.py:12
  216.7 1.4 collective-permute-done.2
  218.1 1.2 fusion.201
  219.3 12.2 %all-reduce = (f32[256]{0:T(256)S(1)}, f32[256]{0:T(256)S(1)}) all-reduce(f32[256]{0:T(256)S(1)} %get-tuple-element.6, f32[256]{0:T(256)S(1)} %get-tuple-element.5), channel_id=1, replica_groups=mesh['sp'=4,'tp'=8] {'tp'}, use_global_device_ids=true, to_apply=%region_14.15 | all-reduce | flops 512 | bytes 4096 | tf_op jit(solution)/shard_map/psum | solution.py:60
  232.5 24.2 %all-gather.17.cloned.1.call-done = bf16[256,2048]{1,0:T(8,128)(2,1)} async-done(((bf16[256,256]{1,0:T(8,128)(2,1)}), bf16[256,2048]{1,0:T(8,128)(2,1)}) %all-gather.17.cloned.1.call-update) | async-done | bytes 1048592 | tf_op jit(solution)/shard_map/all_gather | solution.py:76
  256.6 3.3 %fusion.45 = bf16[256,512]{1,0:T(8,128)(2,1)} fusion(bf16[256,2048]{1,0:T(8,128)(2,1)} %all-gather.17.cloned.1.call-done, bf16[3,2048,512]{2,1,0:T(8,128)(2,1)} %param.17, bf16[256,512]{1,0:T(8,128)(2,1)S(1)} %copy-done.5), kind=kOutput, calls=%fused_computation.132 | convolution fusion | flops 537264128 | bytes 3670016 | tf_op jit(solution)/shard_map/dot_general | solution.py:72
  (47 shorter events, 6.2 us)
Async XLA Ops:
  6.5 33.5 %all-gather.7.cloned.1.call-start = ((), (), s32[]{:S(2)}) async-start(), calls=%async_computation | async-start | bytes 2359296 | tf_op jit(solution)/shard_map/all_gather | solution.py:42
  7.3 84.0 %all-gather.9.cloned.1.call-start = ((), (), s32[]{:S(2)}) async-start(), calls=%async_computation.1 | async-start | bytes 1179648 | tf_op jit(solution)/shard_map/all_gather | solution.py:76
  42.2 3.2 %copy-start = (bf16[256,4096]{1,0:T(8,128)(2,1)S(1)}, bf16[256,4096]{1,0:T(8,128)(2,1)}, u32[]{:S(2)}) copy-start(bf16[256,4096]{1,0:T(8,128)(2,1)} %all-gather.7.cloned.1.call-done) | copy-start | bytes 6291460
  45.3 6.0 %copy-start.7 = (f32[3,256]{1,0:T(4,128)S(1)}, f32[3,256]{1,0:T(4,128)}, u32[]{:S(2)}) copy-start(f32[3,256]{1,0:T(4,128)} %param.16) | copy-start | bytes 9220
  45.4 45.9 %copy-start.3 = (bf16[256,512]{1,0:T(8,128)(2,1)S(1)}, bf16[256,512]{1,0:T(8,128)(2,1)}, u32[]{:S(2)}) copy-start(bf16[256,512]{1,0:T(8,128)(2,1)} %param.9) | copy-start | bytes 786436
  47.8 46.9 %copy-start.6 = (f32[3,31,256]{2,1,0:T(8,128)S(1)}, f32[3,31,256]{2,1,0:T(8,128)}, u32[]{:S(2)}) copy-start(f32[3,31,256]{2,1,0:T(8,128)} %param.13) | copy-start | bytes 285700
  47.9 5.0 %collective-permute-start = (bf16[30,256]{1,0:T(8,128)(2,1)S(1)}, bf16[30,256]{1,0:T(8,128)(2,1)S(1)}, u32[]{:S(2)}, u32[]{:S(2)}) collective-permute-start(bf16[30,256]{1,0:T(8,128)(2,1)S(1)} %slice.1017), channel_id=1, source_target_pairs={{0,8},{8,16},{16,24},{1,9},{9,17},{17,25},{2,10},{10,18},{18,26},{... | collective-permute-start | bytes 46088 | tf_op jit(solution)/shard_map/ppermute | solution.py:12
  67.1 55.8 %all-gather.11.cloned.1.call-start = ((), (), s32[]{:S(2)}) async-start(), calls=%async_computation.2 | async-start | bytes 2359296 | tf_op jit(solution)/shard_map/all_gather | solution.py:42
  94.6 79.3 %all-gather.13.cloned.1.call-start = ((), (), s32[]{:S(2)}) async-start(), calls=%async_computation.3 | async-start | bytes 1179648 | tf_op jit(solution)/shard_map/all_gather | solution.py:76
  125.0 3.2 %copy-start.1 = (bf16[256,4096]{1,0:T(8,128)(2,1)S(1)}, bf16[256,4096]{1,0:T(8,128)(2,1)}, u32[]{:S(2)}) copy-start(bf16[256,4096]{1,0:T(8,128)(2,1)} %all-gather.11.cloned.1.call-done) | copy-start | bytes 6291460
  128.2 45.8 %copy-start.4 = (bf16[256,512]{1,0:T(8,128)(2,1)S(1)}, bf16[256,512]{1,0:T(8,128)(2,1)}, u32[]{:S(2)}) copy-start(bf16[256,512]{1,0:T(8,128)(2,1)} %fusion.51) | copy-start | bytes 786436
  130.7 4.8 %collective-permute-start.1 = (bf16[30,256]{1,0:T(8,128)(2,1)S(1)}, bf16[30,256]{1,0:T(8,128)(2,1)S(1)}, u32[]{:S(2)}, u32[]{:S(2)}) collective-permute-start(bf16[30,256]{1,0:T(8,128)(2,1)S(1)} %slice.1076), channel_id=1, source_target_pairs={{0,8},{8,16},{16,24},{1,9},{9,17},{17,25},{2,10},{10,18},{18,26},{... | collective-permute-start | bytes 46088 | tf_op jit(solution)/shard_map/ppermute | solution.py:12
  149.8 55.8 %all-gather.15.cloned.1.call-start = ((), (), s32[]{:S(2)}) async-start(), calls=%async_computation.4 | async-start | bytes 2359296 | tf_op jit(solution)/shard_map/all_gather | solution.py:42
  177.3 79.3 %all-gather.17.cloned.1.call-start = ((), (), s32[]{:S(2)}) async-start(), calls=%async_computation.5 | async-start | bytes 1179648 | tf_op jit(solution)/shard_map/all_gather | solution.py:76
  207.6 3.2 %copy-start.2 = (bf16[256,4096]{1,0:T(8,128)(2,1)S(1)}, bf16[256,4096]{1,0:T(8,128)(2,1)}, u32[]{:S(2)}) copy-start(bf16[256,4096]{1,0:T(8,128)(2,1)} %all-gather.15.cloned.1.call-done) | copy-start | bytes 6291460
  210.8 45.8 %copy-start.5 = (bf16[256,512]{1,0:T(8,128)(2,1)S(1)}, bf16[256,512]{1,0:T(8,128)(2,1)}, u32[]{:S(2)}) copy-start(bf16[256,512]{1,0:T(8,128)(2,1)} %fusion.48) | copy-start | bytes 786436
  213.3 4.8 %collective-permute-start.2 = (bf16[30,256]{1,0:T(8,128)(2,1)S(1)}, bf16[30,256]{1,0:T(8,128)(2,1)S(1)}, u32[]{:S(2)}, u32[]{:S(2)}) collective-permute-start(bf16[30,256]{1,0:T(8,128)(2,1)S(1)} %slice.1135), channel_id=1, source_target_pairs={{0,8},{8,16},{16,24},{1,9},{9,17},{17,25},{2,10},{10,18},{18,26},{... | collective-permute-start | bytes 46088 | tf_op jit(solution)/shard_map/ppermute | solution.py:12
Sparse Core Ops, SparseCore 0:
  9.2 30.8 all-gather.6
  67.3 23.9 all-gather.8
  94.8 28.0 all-gather.10
  149.9 23.9 all-gather.12
  177.4 28.0 all-gather.14
  232.6 23.9 all-gather.16
where the time goes:
time: 268 us; the launch traced here: 267 us
  waiting for transfers between devices  162 us (60%)
  blocking collectives  36.7 us (14%)
  matrix products  26.8 us (10%)
  between operations  13.7 us (5%)
  other arithmetic  13.3 us (5%)
  starting transfers between devices  10.5 us (4%)
  local copies, waits for them, and re-layouts  3.88 us (1%)
    all_gather x3, waiting for transfers between devices, on_device(): whole_rows = lax.all_gather(current, 'tp', axis=1, tiled=True)  84.5 us
    all_gather x3, waiting for transfers between devices, on_device(): lax.all_gather(hidden, 'tp', axis=1, tiled=True)  72.4 us
    psum x3, blocking collectives, on_device(): lax.psum((jnp.sum(convolved, axis=1), jnp.sum(convolved * convolved, axis...  36.7 us
    dot_general x6, matrix products, against(): lax.dot_general(left, right, (((1,), (1,)), ((), ())), preferred_element_...  16.8 us
    ppermute x3, starting transfers between devices, passed_along(): return lax.ppermute(shard, axis, pairs)  10.3 us
    dot_general x3, matrix products, project_out(): return jnp.dot(block_in, out_matrix, preferred_element_type=jnp.float32)  9.99 us
    reduce_sum x3, other arithmetic, on_device(): jnp.mean(whole_float * whole_float, axis=1, keepdims=True) + EPSILON  6.25 us
  transfers between devices with their start and end apart: 9, of which 9 were waited for; matrix products, arithmetic and copies ran while one was open for 2% of the time, Pallas kernels for 0%

commit v1 on v0

--- a/solution.py
+++ b/solution.py
@@ -73,7 +73,7 @@
 
         projected = project_out(
             jnp.zeros((out_rows, local_width), jnp.float32),
-            lax.all_gather(hidden, "tp", axis=1, tiled=True),
+            jnp.concatenate(lax.all_gather(hidden, "tp"), axis=1),
             jnp.int32(0),
         )
         current = (current.astype(jnp.float32) + projected).astype(jnp.bfloat16)

time: 268 us -> 271 us (1.011)
  local copies, waits for them, and re-layouts: 3.88 us -> 8.3 us
    all_gather x0 -> x3, local copies, waits for them, and re-layouts: none -> 4.42 us  [on_device(): lax.all_gather(hidden, 'tp')]
where the time goes in v1:
time: 271 us; the launch traced here: 270 us
  waiting for transfers between devices  161 us (59%)
  blocking collectives  36.7 us (14%)
  matrix products  25.9 us (10%)
  between operations  13.8 us (5%)
  other arithmetic  13.3 us (5%)
  starting transfers between devices  10.5 us (4%)
  local copies, waits for them, and re-layouts  8.3 us (3%)
    all_gather x3, waiting for transfers between devices, on_device(): whole_rows = lax.all_gather(current, 'tp', axis=1, tiled=True)  84.5 us
    all_gather x3, waiting for transfers between devices, on_device(): lax.all_gather(hidden, 'tp')  72 us
    psum x3, blocking collectives, on_device(): lax.psum((jnp.sum(convolved, axis=1), jnp.sum(convolved * convolved, axis...  36.7 us
    dot_general x6, matrix products, against(): lax.dot_general(left, right, (((1,), (1,)), ((), ())), preferred_element_...  16.8 us
    ppermute x3, starting transfers between devices, passed_along(): return lax.ppermute(shard, axis, pairs)  10.3 us
    dot_general x3, matrix products, project_out(): return jnp.dot(block_in, out_matrix, preferred_element_type=jnp.float32)  9.08 us
    reduce_sum x3, other arithmetic, on_device(): jnp.mean(whole_float * whole_float, axis=1, keepdims=True) + EPSILON  6.25 us
  transfers between devices with their start and end apart: 9, of which 9 were waited for; matrix products, arithmetic and copies ran while one was open for 2% of the time, Pallas kernels for 0%

profile of v1, /device:TPU:0, one launch (start us, length us, event | category | flops | bytes accessed | tf_op | source)
XLA Modules:
  0.0 270.0 jit_solution(7608114176000158147)
XLA Ops:
  12.0 28.1 %all-gather.10.cloned.1.call-done = bf16[256,4096]{1,0:T(8,128)(2,1)} async-done(((bf16[256,512]{1,0:T(8,128)(2,1)}), bf16[256,4096]{1,0:T(8,128)(2,1)}) %all-gather.10.cloned.1.call-update) | async-done | bytes 2097168 | tf_op jit(solution)/shard_map/all_gather | solution.py:42
  40.1 2.1 fusion
  42.2 3.2 %fusion.96 = f32[256,256]{1,0:T(8,128)S(1)} fusion(bf16[3,256,4096]{2,1,0:T(8,128)(2,1)} %param.12, bf16[256,4096]{1,0:T(8,128)(2,1)} %all-gather.10.cloned.1.call-done, f32[4096]{0:T(1024)S(1)} %bitcast.205, f32[256]{0:T(256)S(1)} %add_rsqrt_fusion.5), kind=kOutput, calls=%fused_computation.149 | convolution fusion | flops 541261824 | bytes 4473856 | tf_op jit(solution)/shard_map/dot_general | solution.py:16
  45.4 2.5 fusion.105
  47.9 3.5 %collective-permute-start = (bf16[30,256]{1,0:T(8,128)(2,1)S(1)}, bf16[30,256]{1,0:T(8,128)(2,1)S(1)}, u32[]{:S(2)}, u32[]{:S(2)}) collective-permute-start(bf16[30,256]{1,0:T(8,128)(2,1)S(1)} %slice.1017), channel_id=1, source_target_pairs={{0,8},{8,16},{16,24},{1,9},{9,17},{17,25},{2,10},{10,18},{18,26},{... | collective-permute-start | bytes 46088 | tf_op jit(solution)/shard_map/ppermute | solution.py:12
  51.4 1.4 collective-permute-done
  54.0 12.2 %all-reduce.2 = (f32[256]{0:T(256)S(1)}, f32[256]{0:T(256)S(1)}) all-reduce(f32[256]{0:T(256)S(1)} %get-tuple-element.10, f32[256]{0:T(256)S(1)} %get-tuple-element.9), channel_id=1, replica_groups=mesh['sp'=4,'tp'=8] {'tp'}, use_global_device_ids=true, to_apply=%region_4.0 | all-reduce | flops 512 | bytes 4096 | tf_op jit(solution)/shard_map/psum | solution.py:60
  67.2 24.0 %all-gather.16.cloned.1.call-done = bf16[2048,256]{1,0:T(8,128)(2,1)} async-done(((bf16[256,256]{1,0:T(8,128)(2,1)}), bf16[2048,256]{1,0:T(8,128)(2,1)}) %all-gather.16.cloned.1.call-update) | async-done | bytes 1048592 | tf_op jit(solution)/shard_map/all_gather | solution.py:76
  91.2 1.5 copy.10
  92.7 3.0 %fusion.51 = bf16[256,512]{1,0:T(8,128)(2,1)} fusion(bf16[256,2048]{0,1:T(8,128)(2,1)S(1)} %bitcast.200, bf16[3,2048,512]{2,1,0:T(8,128)(2,1)} %param.17, bf16[256,512]{1,0:T(8,128)(2,1)S(1)} %copy-done.3), kind=kOutput, calls=%fused_computation.134 | convolution fusion | flops 537264128 | bytes 3670016 | tf_op jit(solution)/shard_map/dot_general | solution.py:72
  95.8 28.2 %all-gather.12.cloned.1.call-done = bf16[256,4096]{1,0:T(8,128)(2,1)} async-done(((bf16[256,512]{1,0:T(8,128)(2,1)}), bf16[256,4096]{1,0:T(8,128)(2,1)}) %all-gather.12.cloned.1.call-update) | async-done | bytes 2097168 | tf_op jit(solution)/shard_map/all_gather | solution.py:42
  124.0 2.1 fusion.3
  126.1 3.2 %fusion.93 = f32[256,256]{1,0:T(8,128)S(1)} fusion(bf16[3,256,4096]{2,1,0:T(8,128)(2,1)} %param.12, bf16[256,4096]{1,0:T(8,128)(2,1)} %all-gather.12.cloned.1.call-done, f32[4096]{0:T(1024)S(1)} %bitcast.203, f32[256]{0:T(256)S(1)} %add_rsqrt_fusion.3), kind=kOutput, calls=%fused_computation.148 | convolution fusion | flops 541261824 | bytes 4473856 | tf_op jit(solution)/shard_map/dot_general | solution.py:16
  129.3 2.4 fusion.102
  131.7 3.4 %collective-permute-start.1 = (bf16[30,256]{1,0:T(8,128)(2,1)S(1)}, bf16[30,256]{1,0:T(8,128)(2,1)S(1)}, u32[]{:S(2)}, u32[]{:S(2)}) collective-permute-start(bf16[30,256]{1,0:T(8,128)(2,1)S(1)} %slice.1076), channel_id=1, source_target_pairs={{0,8},{8,16},{16,24},{1,9},{9,17},{17,25},{2,10},{10,18},{18,26},{... | collective-permute-start | bytes 46088 | tf_op jit(solution)/shard_map/ppermute | solution.py:12
  135.2 1.4 collective-permute-done.1
  136.6 1.2 fusion.202
  137.8 12.2 %all-reduce.1 = (f32[256]{0:T(256)S(1)}, f32[256]{0:T(256)S(1)}) all-reduce(f32[256]{0:T(256)S(1)} %get-tuple-element.8, f32[256]{0:T(256)S(1)} %get-tuple-element.7), channel_id=1, replica_groups=mesh['sp'=4,'tp'=8] {'tp'}, use_global_device_ids=true, to_apply=%region_9.10 | all-reduce | flops 512 | bytes 4096 | tf_op jit(solution)/shard_map/psum | solution.py:60
  150.9 24.0 %all-gather.18.cloned.1.call-done = bf16[2048,256]{1,0:T(8,128)(2,1)} async-done(((bf16[256,256]{1,0:T(8,128)(2,1)}), bf16[2048,256]{1,0:T(8,128)(2,1)}) %all-gather.18.cloned.1.call-update) | async-done | bytes 1048592 | tf_op jit(solution)/shard_map/all_gather | solution.py:76
  174.9 1.5 copy.11
  176.4 3.0 %fusion.48 = bf16[256,512]{1,0:T(8,128)(2,1)} fusion(bf16[256,2048]{0,1:T(8,128)(2,1)S(1)} %bitcast.198, bf16[3,2048,512]{2,1,0:T(8,128)(2,1)} %param.17, bf16[256,512]{1,0:T(8,128)(2,1)S(1)} %copy-done.4), kind=kOutput, calls=%fused_computation.133 | convolution fusion | flops 537264128 | bytes 3670016 | tf_op jit(solution)/shard_map/dot_general | solution.py:72
  179.5 28.2 %all-gather.14.cloned.1.call-done = bf16[256,4096]{1,0:T(8,128)(2,1)} async-done(((bf16[256,512]{1,0:T(8,128)(2,1)}), bf16[256,4096]{1,0:T(8,128)(2,1)}) %all-gather.14.cloned.1.call-update) | async-done | bytes 2097168 | tf_op jit(solution)/shard_map/all_gather | solution.py:42
  207.7 2.1 fusion.6
  209.8 3.2 %fusion.90 = f32[256,256]{1,0:T(8,128)S(1)} fusion(bf16[3,256,4096]{2,1,0:T(8,128)(2,1)} %param.12, bf16[256,4096]{1,0:T(8,128)(2,1)} %all-gather.14.cloned.1.call-done, f32[4096]{0:T(1024)S(1)} %bitcast.201, f32[256]{0:T(256)S(1)} %add_rsqrt_fusion.1), kind=kOutput, calls=%fused_computation.147 | convolution fusion | flops 541261824 | bytes 4473856 | tf_op jit(solution)/shard_map/dot_general | solution.py:16
  213.0 2.5 fusion.99
  215.5 3.4 %collective-permute-start.2 = (bf16[30,256]{1,0:T(8,128)(2,1)S(1)}, bf16[30,256]{1,0:T(8,128)(2,1)S(1)}, u32[]{:S(2)}, u32[]{:S(2)}) collective-permute-start(bf16[30,256]{1,0:T(8,128)(2,1)S(1)} %slice.1135), channel_id=1, source_target_pairs={{0,8},{8,16},{16,24},{1,9},{9,17},{17,25},{2,10},{10,18},{18,26},{... | collective-permute-start | bytes 46088 | tf_op jit(solution)/shard_map/ppermute | solution.py:12
  218.9 1.4 collective-permute-done.2
  220.3 1.2 fusion.201
  221.5 12.2 %all-reduce = (f32[256]{0:T(256)S(1)}, f32[256]{0:T(256)S(1)}) all-reduce(f32[256]{0:T(256)S(1)} %get-tuple-element.6, f32[256]{0:T(256)S(1)} %get-tuple-element.5), channel_id=1, replica_groups=mesh['sp'=4,'tp'=8] {'tp'}, use_global_device_ids=true, to_apply=%region_14.15 | all-reduce | flops 512 | bytes 4096 | tf_op jit(solution)/shard_map/psum | solution.py:60
  234.6 24.0 %all-gather.20.cloned.1.call-done = bf16[2048,256]{1,0:T(8,128)(2,1)} async-done(((bf16[256,256]{1,0:T(8,128)(2,1)}), bf16[2048,256]{1,0:T(8,128)(2,1)}) %all-gather.20.cloned.1.call-update) | async-done | bytes 1048592 | tf_op jit(solution)/shard_map/all_gather | solution.py:76
  258.6 1.5 copy.12
  260.1 3.0 %fusion.45 = bf16[256,512]{1,0:T(8,128)(2,1)} fusion(bf16[256,2048]{0,1:T(8,128)(2,1)S(1)} %bitcast.199, bf16[3,2048,512]{2,1,0:T(8,128)(2,1)} %param.17, bf16[256,512]{1,0:T(8,128)(2,1)S(1)} %copy-done.5), kind=kOutput, calls=%fused_computation.132 | convolution fusion | flops 537264128 | bytes 3670016 | tf_op jit(solution)/shard_map/dot_general | solution.py:72
  (50 shorter events, 9.6 us)
Async XLA Ops:
  6.5 33.5 %all-gather.10.cloned.1.call-start = ((), (), s32[]{:S(2)}) async-start(), calls=%async_computation | async-start | bytes 2359296 | tf_op jit(solution)/shard_map/all_gather | solution.py:42
  7.3 83.9 %all-gather.16.cloned.1.call-start = ((), (), s32[]{:S(2)}) async-start(), calls=%async_computation.3 | async-start | bytes 1179648 | tf_op jit(solution)/shard_map/all_gather | solution.py:76
  42.2 3.2 %copy-start = (bf16[256,4096]{1,0:T(8,128)(2,1)S(1)}, bf16[256,4096]{1,0:T(8,128)(2,1)}, u32[]{:S(2)}) copy-start(bf16[256,4096]{1,0:T(8,128)(2,1)} %all-gather.10.cloned.1.call-done) | copy-start | bytes 6291460
  45.3 6.0 %copy-start.7 = (f32[3,256]{1,0:T(4,128)S(1)}, f32[3,256]{1,0:T(4,128)}, u32[]{:S(2)}) copy-start(f32[3,256]{1,0:T(4,128)} %param.16) | copy-start | bytes 9220
  45.4 47.3 %copy-start.3 = (bf16[256,512]{1,0:T(8,128)(2,1)S(1)}, bf16[256,512]{1,0:T(8,128)(2,1)}, u32[]{:S(2)}) copy-start(bf16[256,512]{1,0:T(8,128)(2,1)} %param.9) | copy-start | bytes 786436
  47.8 47.9 %copy-start.6 = (f32[3,31,256]{2,1,0:T(8,128)S(1)}, f32[3,31,256]{2,1,0:T(8,128)}, u32[]{:S(2)}) copy-start(f32[3,31,256]{2,1,0:T(8,128)} %param.13) | copy-start | bytes 285700
  47.9 5.0 %collective-permute-start = (bf16[30,256]{1,0:T(8,128)(2,1)S(1)}, bf16[30,256]{1,0:T(8,128)(2,1)S(1)}, u32[]{:S(2)}, u32[]{:S(2)}) collective-permute-start(bf16[30,256]{1,0:T(8,128)(2,1)S(1)} %slice.1017), channel_id=1, source_target_pairs={{0,8},{8,16},{16,24},{1,9},{9,17},{17,25},{2,10},{10,18},{18,26},{... | collective-permute-start | bytes 46088 | tf_op jit(solution)/shard_map/ppermute | solution.py:12
  67.1 56.8 %all-gather.12.cloned.1.call-start = ((), (), s32[]{:S(2)}) async-start(), calls=%async_computation.1 | async-start | bytes 2359296 | tf_op jit(solution)/shard_map/all_gather | solution.py:42
  95.7 79.2 %all-gather.18.cloned.1.call-start = ((), (), s32[]{:S(2)}) async-start(), calls=%async_computation.4 | async-start | bytes 1179648 | tf_op jit(solution)/shard_map/all_gather | solution.py:76
  126.1 3.2 %copy-start.1 = (bf16[256,4096]{1,0:T(8,128)(2,1)S(1)}, bf16[256,4096]{1,0:T(8,128)(2,1)}, u32[]{:S(2)}) copy-start(bf16[256,4096]{1,0:T(8,128)(2,1)} %all-gather.12.cloned.1.call-done) | copy-start | bytes 6291460
  129.3 47.1 %copy-start.4 = (bf16[256,512]{1,0:T(8,128)(2,1)S(1)}, bf16[256,512]{1,0:T(8,128)(2,1)}, u32[]{:S(2)}) copy-start(bf16[256,512]{1,0:T(8,128)(2,1)} %fusion.51) | copy-start | bytes 786436
  131.7 4.8 %collective-permute-start.1 = (bf16[30,256]{1,0:T(8,128)(2,1)S(1)}, bf16[30,256]{1,0:T(8,128)(2,1)S(1)}, u32[]{:S(2)}, u32[]{:S(2)}) collective-permute-start(bf16[30,256]{1,0:T(8,128)(2,1)S(1)} %slice.1076), channel_id=1, source_target_pairs={{0,8},{8,16},{16,24},{1,9},{9,17},{17,25},{2,10},{10,18},{18,26},{... | collective-permute-start | bytes 46088 | tf_op jit(solution)/shard_map/ppermute | solution.py:12
  150.9 56.8 %all-gather.14.cloned.1.call-start = ((), (), s32[]{:S(2)}) async-start(), calls=%async_computation.2 | async-start | bytes 2359296 | tf_op jit(solution)/shard_map/all_gather | solution.py:42
  179.4 79.2 %all-gather.20.cloned.1.call-start = ((), (), s32[]{:S(2)}) async-start(), calls=%async_computation.5 | async-start | bytes 1179648 | tf_op jit(solution)/shard_map/all_gather | solution.py:76
  209.8 3.2 %copy-start.2 = (bf16[256,4096]{1,0:T(8,128)(2,1)S(1)}, bf16[256,4096]{1,0:T(8,128)(2,1)}, u32[]{:S(2)}) copy-start(bf16[256,4096]{1,0:T(8,128)(2,1)} %all-gather.14.cloned.1.call-done) | copy-start | bytes 6291460
  213.0 47.1 %copy-start.5 = (bf16[256,512]{1,0:T(8,128)(2,1)S(1)}, bf16[256,512]{1,0:T(8,128)(2,1)}, u32[]{:S(2)}) copy-start(bf16[256,512]{1,0:T(8,128)(2,1)} %fusion.48) | copy-start | bytes 786436
  215.5 4.8 %collective-permute-start.2 = (bf16[30,256]{1,0:T(8,128)(2,1)S(1)}, bf16[30,256]{1,0:T(8,128)(2,1)S(1)}, u32[]{:S(2)}, u32[]{:S(2)}) collective-permute-start(bf16[30,256]{1,0:T(8,128)(2,1)S(1)} %slice.1135), channel_id=1, source_target_pairs={{0,8},{8,16},{16,24},{1,9},{9,17},{17,25},{2,10},{10,18},{18,26},{... | collective-permute-start | bytes 46088 | tf_op jit(solution)/shard_map/ppermute | solution.py:12
Sparse Core Ops, SparseCore 0:
  9.2 30.8 all-gather.9
  67.3 23.8 all-gather.15
  95.8 28.0 all-gather.11
  151.0 23.8 all-gather.17
  179.6 28.0 all-gather.13
  234.7 23.8 all-gather.19
